TPU v7x, 32 devices: a whole 2x2x4 slice. The times are simulated.
32 devices in a mesh: kv: 8 (over z, y), tp: 4 (over x, core).
Axes of the slice: x: 2, y: 2, z: 4, core: 2. Of those that a mesh axis runs over, the one named last changes fastest.
Arguments:
- tokens: bfloat16 [4096, 2048], P('kv'), may hold values from -18 to 18
- w_query: bfloat16 [2048, 1024], P(None, 'tp'), may hold values from -0.125 to 0.125
- w_key: bfloat16 [2048, 256], P(None, 'tp'), may hold values from -0.125 to 0.125
- w_value: bfloat16 [2048, 256], P(None, 'tp'), may hold values from -18 to 18
- w_out: bfloat16 [1024, 2048], P(None, 'tp'), may hold values from -0.1875 to 0.1875
- out_gain: float32 [1024], replicated, may hold values from 0.1 to 1.9
- chosen: int32 [4, 64, 8], P('tp', 'kv'), may hold values from -1 to 63, as said below
Outputs:
- mixed_out: bfloat16 [4096, 2048], P('kv', 'tp')
Inputs may be any that keep to these rules, and one draw needn't show every extreme that they name: chosen[h, b, 0] is b itself; the other entries of a row are distinct key blocks lying wholly before block b, or -1, placed after all named blocks; for each key head h, the query blocks on one index of kv (its 512 positions) name, together, at most one key block of head h held by any other index of kv.
All inputs are finite; a program needn't handle non-finite values.
Results may differ from a plain program's by a relative error of at most 0.024.
Values may be sent and summed in bfloat16 or wider, within the bound.
No kernel may reach another device: no remote copies, remote signals or barrier semaphores. Data moves between devices by JAX's collectives and lax.ppermute only.
A program may use at most 64 MiB of HBM per device.

v0:
```python
import jax
import jax.numpy as jnp
from jax import lax
from jax.sharding import PartitionSpec as P

HQ = 16
HD = 64
BLK = 64
SEL = 8
rope_base = 500000.0
norm_eps = 1e-06


def rotate(vectors, positions):
    half_size = vectors.shape[-1] // 2
    frequency = rope_base ** (-jnp.arange(half_size, dtype=jnp.float32) / half_size)
    angles = positions.astype(jnp.float32)[:, None] * frequency[None, :]
    cosine = jnp.cos(angles)[:, None, :]
    sine_wave = jnp.sin(angles)[:, None, :]
    lower_half = vectors[..., :half_size]
    upper_half = vectors[..., half_size:]
    return jnp.concatenate(
        [
            lower_half * cosine - upper_half * sine_wave,
            upper_half * cosine + lower_half * sine_wave,
        ],
        axis=-1,
    )


def per_device(tokens, w_query, w_key, w_value, w_out, out_gain, chosen):
    count_kv = lax.axis_size("kv")
    kv_place = lax.axis_index("kv")
    row_count = tokens.shape[0]
    block_count = row_count // BLK
    feat_width = w_query.shape[1]
    head_count = feat_width // HD
    positions = kv_place * row_count + jnp.arange(row_count, dtype=jnp.int32)
    queries = rotate(
        jnp.dot(tokens, w_query, preferred_element_type=jnp.float32).reshape(
            row_count, head_count, HD
        ),
        positions,
    ).astype(jnp.bfloat16)
    key_rows = (
        rotate(
            jnp.dot(tokens, w_key, preferred_element_type=jnp.float32).reshape(row_count, 1, HD),
            positions,
        )
        .astype(jnp.bfloat16)
        .reshape(row_count, HD)
    )
    value_rows = jnp.dot(tokens, w_value, preferred_element_type=jnp.float32).astype(jnp.bfloat16)
    local_pairs = jnp.concatenate([key_rows, value_rows], axis=1).reshape(block_count, BLK, 2 * HD)
    chosen_ids = chosen[0]
    usable = chosen_ids >= 0
    owners = jnp.where(usable, chosen_ids // block_count, kv_place)
    local_index = jnp.where(usable, chosen_ids % block_count, 0)
    remote = usable & (owners != kv_place)
    peer_ids = jnp.arange(count_kv, dtype=jnp.int32)
    matches = remote[:, :, None] & (owners[:, :, None] == peer_ids[None, None, :])
    wanted = jnp.max(jnp.where(matches, local_index[:, :, None], -1), axis=(0, 1))
    asked_for = lax.all_to_all(
        wanted.reshape(count_kv, 1), "kv", split_axis=0, concat_axis=0, tiled=True
    )[:, 0]
    outgoing = jnp.where(
        (asked_for >= 0)[:, None, None],
        local_pairs[jnp.maximum(asked_for, 0)],
        jnp.zeros((), jnp.bfloat16),
    )
    arrived = lax.all_to_all(outgoing, "kv", split_axis=0, concat_axis=0, tiled=True)
    pool_pairs = jnp.concatenate([arrived, local_pairs], axis=0)
    slot_index = jnp.where(owners == kv_place, count_kv + local_index, owners)
    selected = pool_pairs[slot_index]
    pair_count = block_count // 2
    offsets = jnp.arange(BLK, dtype=jnp.int32)
    score_scale = HD ** (-0.5)

    def attend(bundle):
        query_part, stacked, pair_ids, pair_usable, query_pos = bundle
        key_part = stacked[..., :HD]
        value_part = stacked[..., HD:]
        scores = (
            jnp.einsum("pqhd,pskd->phqsk", query_part, key_part, preferred_element_type=jnp.float32)
            * score_scale
        )
        key_pos = pair_ids[:, :, None] * BLK + offsets
        allowed = pair_usable[:, None, :, None] & (
            key_pos[:, None, :, :] <= query_pos[:, :, None, None]
        )
        scores = jnp.where(allowed[:, None], scores, -jnp.inf)
        peak_score = jnp.max(scores, axis=(3, 4), keepdims=True)
        weights = jnp.exp(scores - peak_score)
        softmax_w = (weights / jnp.sum(weights, axis=(3, 4), keepdims=True)).astype(jnp.bfloat16)
        mixed_out = jnp.einsum(
            "phqsk,pskd->pqhd", softmax_w, value_part, preferred_element_type=jnp.float32
        )
        return mixed_out.astype(jnp.bfloat16)

    attended = lax.map(
        attend,
        (
            queries.reshape(pair_count, 2, BLK, head_count, HD),
            selected.reshape(pair_count, 2, SEL, BLK, 2 * HD),
            chosen_ids.reshape(pair_count, 2, SEL),
            usable.reshape(pair_count, 2, SEL),
            positions.reshape(pair_count, 2, BLK),
        ),
    ).reshape(row_count, feat_width)
    attn_f32 = attended.astype(jnp.float32)
    squares = lax.psum(jnp.sum(attn_f32 * attn_f32, axis=1), "tp")
    gain_part = lax.dynamic_slice_in_dim(out_gain, lax.axis_index("tp") * feat_width, feat_width)
    scaled = (attn_f32 * gain_part[None, :]).astype(jnp.bfloat16)
    product = jnp.dot(
        lax.all_gather(scaled, "tp", axis=1, tiled=True), w_out, preferred_element_type=jnp.float32
    )
    inverse = lax.rsqrt(squares / (HQ * HD) + norm_eps)
    return (inverse[:, None] * product).astype(jnp.bfloat16)


def solution(mesh):
    return jax.shard_map(
        per_device,
        mesh=mesh,
        in_specs=(
            P("kv", None),
            P(None, "tp"),
            P(None, "tp"),
            P(None, "tp"),
            P(None, "tp"),
            P(),
            P("tp", "kv", None),
        ),
        out_specs=P("kv", "tp"),
        check_vma=False,
    )
```

profile of v0, /device:TPU:0, one launch (start us, length us, event | category | flops | bytes accessed | tf_op | source)
XLA Modules:
  0.0 87.1 jit_solution(12271367534152278380)
XLA Ops:
  6.5 0.8 fusion.20
  8.9 7.3 %all-to-all-start = ((s32[8,1,1]{2,1,0:T(1,128)}), s32[8,1,1]{2,1,0:T(1,128)S(1)}, u32[]{:S(2)}, u32[]{:S(2)}) async-start(s32[8,1,1]{2,1,0:T(1,128)} %copy.36), calls=%async_computation | async-start | bytes 8192 | tf_op jit(solution)/shard_map/all_to_all | solution.py:63
  16.9 1.7 %convolution_bitcast_fusion.1 = f32[512,1,64]{0,2,1:T(8,128)S(1)} fusion(bf16[512,2048]{1,0:T(8,128)(2,1)S(1)} %copy-done, bf16[2048,64]{0,1:T(8,128)(2,1)} %param.11), kind=kOutput, calls=%fused_computation.26 | convolution fusion | flops 134217728 | bytes 2490368 | tf_op jit(solution)/shard_map/dot_general | solution.py:47
  20.4 2.0 %fusion.34 = f32[512,256]{0,1:T(8,128)S(1)} fusion(bf16[512,2048]{1,0:T(8,128)(2,1)S(1)} %copy-done, bf16[2048,256]{1,0:T(8,128)(2,1)} %param.10), kind=kOutput, calls=%fused_computation.93 | convolution fusion | flops 536870912 | bytes 3670016 | tf_op jit(solution)/shard_map/dot_general | solution.py:40
  22.9 1.6 %pad_maximum_fusion = bf16[4,2,64,4,64]{2,1,0,4,3:T(2,128)(2,1)} fusion(bf16[4,2,64,4,32]{2,1,0,4,3:T(2,128)(2,1)S(1)} %concatenate.35, bf16[4,2,64,4,32]{2,1,0,4,3:T(2,128)(2,1)S(1)} %concatenate.34), kind=kLoop, calls=%fused_computation.29 | loop fusion | flops 131072 | bytes 524288 | tf_op jit(solution)/shard_map/concatenate | solution.py:22
  26.6 6.0 %all-to-all-start.1 = ((bf16[8,64,128]{2,1,0:T(8,128)(2,1)}), bf16[8,64,128]{2,1,0:T(8,128)(2,1)S(1)}, u32[]{:S(2)}, u32[]{:S(2)}) async-start(bf16[8,64,128]{2,1,0:T(8,128)(2,1)} %broadcast_select_fusion), calls=%async_computation.1 | async-start | bytes 262144 | tf_op jit(solution)/shard_map/all_to_all | solution.py:71
  32.7 0.8 dynamic_slice.23
  33.4 6.5 %all-to-all-done.1 = bf16[8,64,128]{2,1,0:T(8,128)(2,1)S(1)} async-done(((bf16[8,64,128]{2,1,0:T(8,128)(2,1)}), bf16[8,64,128]{2,1,0:T(8,128)(2,1)S(1)}, u32[]{:S(2)}, u32[]{:S(2)}) %all-to-all-start.1) | async-done | bytes 131104 | tf_op jit(solution)/shard_map/all_to_all | solution.py:71
  40.8 17.1 %while.11 = (s32[]{:T(128)}, bf16[4,2,64,4,64]{2,4,3,1,0:T(8,128)(2,1)}, bf16[4,2,8,64,128]{4,3,2,1,0:T(8,128)(2,1)S(1)}, pred[4,2,8]{2,1,0:T(4,128)(4,1)S(1)}, ...) while((s32[]{:T(128)}, ...), condition=%wide.region_4.5_spmd.clone, body=%wide.region_1.4_spmd.clone.sunk | while | flops 69369872 | bytes 13193617 | solution.py:100
  41.8 1.0 %constant_dynamic-slice_fusion.4 = bf16[1,2,64,4,64]{2,1,0,4,3:T(2,128)(2,1)S(1)} fusion(bf16[4,2,64,4,64]{2,1,0,4,3:T(2,128)(2,1)} %get-tuple-element.185, s32[]{:T(128)} %get-tuple-element.171), kind=kLoop, calls=%fused_computation.18.clone.1 | loop fusion | bytes 131076 | tf_op jit(solution)/shard_map/while/body/jit(dynamic_index_in_dim)/dynamic_slice | solution.py:100
  43.9 1.2 %fusion.52 = bf16[4,2,64,4,64]{2,4,3,1,0:T(8,128)(2,1)} fusion(bf16[4,2,64,4,64]{2,4,3,1,0:T(8,128)(2,1)} %get-tuple-element.172, s32[]{:T(128)} %get-tuple-element.171, f32[2,4,64,8,64]{2,4,1,3,0:T(8,128)S(1)} %get-tuple-element.161, f32[2,4,64]{2,1,0:T(4,128)S(1)} %fusion.51, f32[2,4,64]{2,1,0:T(4,128)S(1)} %get-tuple-element.162, ...), kind=kOutput, calls=%fused_computation.10.clone.1 | convolution fusion | flops 34373632 | bytes 1446400 | tf_op jit(solution)/shard_map/while/body/eval_jaxpr/phqsk,pskd->pqhd/dot_general | solution.py:95
  46.1 1.0 %constant_dynamic-slice_fusion.4 = bf16[1,2,64,4,64]{2,1,0,4,3:T(2,128)(2,1)S(1)} fusion(bf16[4,2,64,4,64]{2,1,0,4,3:T(2,128)(2,1)} %get-tuple-element.185, s32[]{:T(128)} %get-tuple-element.171), kind=kLoop, calls=%fused_computation.18.clone.1 | loop fusion | bytes 131076 | tf_op jit(solution)/shard_map/while/body/jit(dynamic_index_in_dim)/dynamic_slice | solution.py:100
  48.1 1.2 %fusion.52 = bf16[4,2,64,4,64]{2,4,3,1,0:T(8,128)(2,1)} fusion(bf16[4,2,64,4,64]{2,4,3,1,0:T(8,128)(2,1)} %get-tuple-element.172, s32[]{:T(128)} %get-tuple-element.171, f32[2,4,64,8,64]{2,4,1,3,0:T(8,128)S(1)} %get-tuple-element.161, f32[2,4,64]{2,1,0:T(4,128)S(1)} %fusion.51, f32[2,4,64]{2,1,0:T(4,128)S(1)} %get-tuple-element.162, ...), kind=kOutput, calls=%fused_computation.10.clone.1 | convolution fusion | flops 34373632 | bytes 1446400 | tf_op jit(solution)/shard_map/while/body/eval_jaxpr/phqsk,pskd->pqhd/dot_general | solution.py:95
  50.4 1.0 %constant_dynamic-slice_fusion.4 = bf16[1,2,64,4,64]{2,1,0,4,3:T(2,128)(2,1)S(1)} fusion(bf16[4,2,64,4,64]{2,1,0,4,3:T(2,128)(2,1)} %get-tuple-element.185, s32[]{:T(128)} %get-tuple-element.171), kind=kLoop, calls=%fused_computation.18.clone.1 | loop fusion | bytes 131076 | tf_op jit(solution)/shard_map/while/body/jit(dynamic_index_in_dim)/dynamic_slice | solution.py:100
  52.4 1.2 %fusion.52 = bf16[4,2,64,4,64]{2,4,3,1,0:T(8,128)(2,1)} fusion(bf16[4,2,64,4,64]{2,4,3,1,0:T(8,128)(2,1)} %get-tuple-element.172, s32[]{:T(128)} %get-tuple-element.171, f32[2,4,64,8,64]{2,4,1,3,0:T(8,128)S(1)} %get-tuple-element.161, f32[2,4,64]{2,1,0:T(4,128)S(1)} %fusion.51, f32[2,4,64]{2,1,0:T(4,128)S(1)} %get-tuple-element.162, ...), kind=kOutput, calls=%fused_computation.10.clone.1 | convolution fusion | flops 34373632 | bytes 1446400 | tf_op jit(solution)/shard_map/while/body/eval_jaxpr/phqsk,pskd->pqhd/dot_general | solution.py:95
  54.7 1.0 %constant_dynamic-slice_fusion.4 = bf16[1,2,64,4,64]{2,1,0,4,3:T(2,128)(2,1)S(1)} fusion(bf16[4,2,64,4,64]{2,1,0,4,3:T(2,128)(2,1)} %get-tuple-element.185, s32[]{:T(128)} %get-tuple-element.171), kind=kLoop, calls=%fused_computation.18.clone.1 | loop fusion | bytes 131076 | tf_op jit(solution)/shard_map/while/body/jit(dynamic_index_in_dim)/dynamic_slice | solution.py:100
  56.7 1.2 %fusion.52 = bf16[4,2,64,4,64]{2,4,3,1,0:T(8,128)(2,1)} fusion(bf16[4,2,64,4,64]{2,4,3,1,0:T(8,128)(2,1)} %get-tuple-element.172, s32[]{:T(128)} %get-tuple-element.171, f32[2,4,64,8,64]{2,4,1,3,0:T(8,128)S(1)} %get-tuple-element.161, f32[2,4,64]{2,1,0:T(4,128)S(1)} %fusion.51, f32[2,4,64]{2,1,0:T(4,128)S(1)} %get-tuple-element.162, ...), kind=kOutput, calls=%fused_computation.10.clone.1 | convolution fusion | flops 34373632 | bytes 1446400 | tf_op jit(solution)/shard_map/while/body/eval_jaxpr/phqsk,pskd->pqhd/dot_general | solution.py:95
  57.9 1.3 %copy.41 = f32[4,2,64,4,64]{4,3,2,1,0:T(4,128)S(1)} copy(bf16[4,2,64,4,64]{2,4,3,1,0:T(8,128)(2,1)} %get-tuple-element.47) | data formatting | bytes 786432 | tf_op jit(solution)/shard_map/convert_element_type | solution.py:110
  59.3 1.4 %reshape.350 = f32[512,256]{1,0:T(8,128)} reshape(f32[4,2,64,4,64]{4,3,2,1,0:T(4,128)S(1)} %copy.41) | data formatting | bytes 1048576 | tf_op jit(solution)/shard_map/convert_element_type | solution.py:110
  60.7 1.8 %multiply_convert_fusion = bf16[512,256]{1,0:T(8,128)(2,1)} fusion(f32[512,256]{1,0:T(8,128)} %reshape.350, f32[256]{0:T(256)S(1)} %dynamic_slice.23), kind=kLoop, calls=%fused_computation.30 | loop fusion | flops 262144 | bytes 787456 | tf_op jit(solution)/shard_map/convert_element_type | solution.py:113
  62.5 1.2 %multiply_reduce_fusion = f32[4,2,64]{2,1,0:T(2,128)S(1)} fusion(bf16[4,2,64,4,64]{2,4,3,1,0:T(8,128)(2,1)} %get-tuple-element.47), kind=kLoop, calls=%fused_computation.28 | loop fusion | flops 392704 | bytes 264192 | tf_op jit(solution)/shard_map/reduce_sum | solution.py:111
  63.8 5.6 %psum.7 = f32[512]{0:T(512)S(1)} all-reduce(f32[512]{0:T(512)S(1)} %reduce_sum.21), channel_id=1, replica_groups=mesh['kv'=8,'tp'=4] {'tp'}, use_global_device_ids=true, to_apply=%region_6.7 | all-reduce | flops 512 | bytes 4096 | tf_op jit(solution)/shard_map/psum | solution.py:111
  69.4 7.8 %all-gather.2.cloned.1.call-done = bf16[512,1024]{1,0:T(8,128)(2,1)} async-done(((bf16[512,256]{1,0:T(8,128)(2,1)}), bf16[512,1024]{1,0:T(8,128)(2,1)}) %all-gather.2.cloned.1.call-update) | async-done | bytes 1048592 | tf_op jit(solution)/shard_map/all_gather | solution.py:115
  77.3 3.0 %fusion.10 = bf16[512,512]{1,0:T(8,128)(2,1)} fusion(bf16[512,1024]{1,0:T(8,128)(2,1)} %all-gather.2.cloned.1.call-done, bf16[1024,512]{1,0:T(8,128)(2,1)} %param.13, f32[512]{0:T(512)S(1)} %add_rsqrt_fusion), kind=kOutput, calls=%fused_computation.25 | convolution fusion | flops 537395200 | bytes 2623488 | tf_op jit(solution)/shard_map/dot_general | solution.py:114
  (91 shorter events, 15.5 us)
Async XLA Ops:
  6.5 10.4 %copy-start = (bf16[512,2048]{1,0:T(8,128)(2,1)S(1)}, bf16[512,2048]{1,0:T(8,128)(2,1)}, u32[]{:S(2)}) copy-start(bf16[512,2048]{1,0:T(8,128)(2,1)} %param.9) | copy-start | bytes 6291460
  6.5 13.0 %copy-start.3 = (bf16[2048,64]{0,1:T(8,128)(2,1)S(1)}, bf16[2048,64]{0,1:T(8,128)(2,1)}, u32[]{:S(2)}) copy-start(bf16[2048,64]{0,1:T(8,128)(2,1)} %param.12) | copy-start | bytes 786436
  8.9 15.9 %all-to-all-start = ((s32[8,1,1]{2,1,0:T(1,128)}), s32[8,1,1]{2,1,0:T(1,128)S(1)}, u32[]{:S(2)}, u32[]{:S(2)}) async-start(s32[8,1,1]{2,1,0:T(1,128)} %copy.36), calls=%async_computation | async-start | bytes 8192 | tf_op jit(solution)/shard_map/all_to_all | solution.py:63
  22.4 11.0 %copy-start.4 = (s32[1,8,8]{2,1,0:T(8,128)S(1)}, s32[1,8,8]{2,1,0:T(8,128)}, u32[]{:S(2)}) copy-start(s32[1,8,8]{2,1,0:T(8,128)} %param.15) | copy-start | bytes 772
  26.6 13.3 %all-to-all-start.1 = ((bf16[8,64,128]{2,1,0:T(8,128)(2,1)}), bf16[8,64,128]{2,1,0:T(8,128)(2,1)S(1)}, u32[]{:S(2)}, u32[]{:S(2)}) async-start(bf16[8,64,128]{2,1,0:T(8,128)(2,1)} %broadcast_select_fusion), calls=%async_computation.1 | async-start | bytes 262144 | tf_op jit(solution)/shard_map/all_to_all | solution.py:71
  32.6 44.7 %all-gather.2.cloned.1.call-start = ((), (), s32[]{:S(2)}) async-start(), calls=%async_computation.2 | async-start | bytes 1310720 | tf_op jit(solution)/shard_map/all_gather | solution.py:115
  40.8 1.0 %copy-start.1 = (bf16[4,2,8,64,128]{4,3,2,1,0:T(8,128)(2,1)}, bf16[4,2,8,64,128]{4,3,2,1,0:T(8,128)(2,1)S(1)}, u32[]{:S(2)}) copy-start(bf16[4,2,8,64,128]{4,3,2,1,0:T(8,128)(2,1)S(1)} %get-tuple-element.181) | copy-start | bytes 3145732 | tf_op jit(solution)/shard_map/while
  43.9 1.2 %copy-start.2 = (bf16[4,2,8,64,128]{4,3,2,1,0:T(8,128)(2,1)S(1)}, bf16[4,2,8,64,128]{4,3,2,1,0:T(8,128)(2,1)}, u32[]{:S(2)}) copy-start(bf16[4,2,8,64,128]{4,3,2,1,0:T(8,128)(2,1)} %copy-done.1) | copy-start | bytes 3145732 | tf_op jit(solution)/shard_map/while
  45.1 1.0 %copy-start.1 = (bf16[4,2,8,64,128]{4,3,2,1,0:T(8,128)(2,1)}, bf16[4,2,8,64,128]{4,3,2,1,0:T(8,128)(2,1)S(1)}, u32[]{:S(2)}) copy-start(bf16[4,2,8,64,128]{4,3,2,1,0:T(8,128)(2,1)S(1)} %get-tuple-element.181) | copy-start | bytes 3145732 | tf_op jit(solution)/shard_map/while
  48.1 1.2 %copy-start.2 = (bf16[4,2,8,64,128]{4,3,2,1,0:T(8,128)(2,1)S(1)}, bf16[4,2,8,64,128]{4,3,2,1,0:T(8,128)(2,1)}, u32[]{:S(2)}) copy-start(bf16[4,2,8,64,128]{4,3,2,1,0:T(8,128)(2,1)} %copy-done.1) | copy-start | bytes 3145732 | tf_op jit(solution)/shard_map/while
  49.4 1.0 %copy-start.1 = (bf16[4,2,8,64,128]{4,3,2,1,0:T(8,128)(2,1)}, bf16[4,2,8,64,128]{4,3,2,1,0:T(8,128)(2,1)S(1)}, u32[]{:S(2)}) copy-start(bf16[4,2,8,64,128]{4,3,2,1,0:T(8,128)(2,1)S(1)} %get-tuple-element.181) | copy-start | bytes 3145732 | tf_op jit(solution)/shard_map/while
  52.4 1.2 %copy-start.2 = (bf16[4,2,8,64,128]{4,3,2,1,0:T(8,128)(2,1)S(1)}, bf16[4,2,8,64,128]{4,3,2,1,0:T(8,128)(2,1)}, u32[]{:S(2)}) copy-start(bf16[4,2,8,64,128]{4,3,2,1,0:T(8,128)(2,1)} %copy-done.1) | copy-start | bytes 3145732 | tf_op jit(solution)/shard_map/while
  53.7 1.0 %copy-start.1 = (bf16[4,2,8,64,128]{4,3,2,1,0:T(8,128)(2,1)}, bf16[4,2,8,64,128]{4,3,2,1,0:T(8,128)(2,1)S(1)}, u32[]{:S(2)}) copy-start(bf16[4,2,8,64,128]{4,3,2,1,0:T(8,128)(2,1)S(1)} %get-tuple-element.181) | copy-start | bytes 3145732 | tf_op jit(solution)/shard_map/while
  56.7 1.2 %copy-start.2 = (bf16[4,2,8,64,128]{4,3,2,1,0:T(8,128)(2,1)S(1)}, bf16[4,2,8,64,128]{4,3,2,1,0:T(8,128)(2,1)}, u32[]{:S(2)}) copy-start(bf16[4,2,8,64,128]{4,3,2,1,0:T(8,128)(2,1)} %copy-done.1) | copy-start | bytes 3145732 | tf_op jit(solution)/shard_map/while
Sparse Core Ops, SparseCore 0:
  62.6 14.5 all-gather.1
where the time goes:
time: 87.9 us; the launch traced here: 87.1 us
  matrix products  14.5 us (16%)
  waiting for transfers between devices  14.3 us (16%)
  local copies, waits for them, and re-layouts  13.6 us (15%)
  between operations  13.6 us (15%)
  starting transfers between devices  13.3 us (15%)
  other arithmetic  11.9 us (14%)
  blocking collectives  5.63 us (6%)
    all_gather x1, waiting for transfers between devices, per_device(): lax.all_gather(scaled, 'tp', axis=1, tiled=True)  7.83 us
    all_to_all x1, starting transfers between devices, per_device(): lax.all_to_all(wanted.reshape(count_kv, 1), 'kv', split_axis=0, concat_ax...  7.31 us
    all_to_all x1, waiting for transfers between devices, per_device(): lax.all_to_all(outgoing, 'kv', split_axis=0, concat_axis=0, tiled=True)  6.5 us
    all_to_all x1, starting transfers between devices, per_device(): lax.all_to_all(outgoing, 'kv', split_axis=0, concat_axis=0, tiled=True)  6 us
    psum x1, blocking collectives, per_device(): squares = lax.psum(jnp.sum(attn_f32 * attn_f32, axis=1), 'tp')  5.63 us
    dot_general x4, matrix products, attend(): jnp.einsum('phqsk,pskd->pqhd', softmax_w, value_part, preferred_element_t...  4.94 us
    dynamic_slice x8, local copies, waits for them, and re-layouts, per_device(): lax.map(attend, (queries.reshape(pair_count, 2, BLK, head_count, HD), sel...  4.53 us
    dot_general x1, matrix products, per_device(): jnp.dot(lax.all_gather(scaled, 'tp', axis=1, tiled=True), w_out, preferre...  3.04 us
  transfers between devices with their start and end apart: 3, of which 2 were waited for; matrix products, arithmetic and copies ran while one was open for 12% of the time, Pallas kernels for 0%

commit v1 on v0

--- a/solution.py
+++ b/solution.py
@@ -9,6 +9,11 @@
 SEL = 8
 rope_base = 500000.0
 norm_eps = 1e-06
+
+
+def gather_blocks(x, axis, dim):
+    parts = lax.all_gather(x, axis)
+    return jnp.concatenate(parts, axis=dim)
 
 
 def rotate(vectors, positions):
@@ -111,9 +116,7 @@
     squares = lax.psum(jnp.sum(attn_f32 * attn_f32, axis=1), "tp")
     gain_part = lax.dynamic_slice_in_dim(out_gain, lax.axis_index("tp") * feat_width, feat_width)
     scaled = (attn_f32 * gain_part[None, :]).astype(jnp.bfloat16)
-    product = jnp.dot(
-        lax.all_gather(scaled, "tp", axis=1, tiled=True), w_out, preferred_element_type=jnp.float32
-    )
+    product = jnp.dot(gather_blocks(scaled, "tp", 1), w_out, preferred_element_type=jnp.float32)
     inverse = lax.rsqrt(squares / (HQ * HD) + norm_eps)
     return (inverse[:, None] * product).astype(jnp.bfloat16)
 

time: 87.9 us -> 89 us (1.013)
  local copies, waits for them, and re-layouts: 13.6 us -> 15.1 us
    all_gather x0 -> x1, local copies, waits for them, and re-layouts: none -> 1.49 us  [gather_blocks(): parts = lax.all_gather(x, axis)]
where the time goes in v1:
time: 89 us; the launch traced here: 88.2 us
  local copies, waits for them, and re-layouts  15.1 us (17%)
  matrix products  14.3 us (16%)
  waiting for transfers between devices  14.2 us (16%)
  between operations  13.6 us (15%)
  starting transfers between devices  13.3 us (15%)
  other arithmetic  11.9 us (13%)
  blocking collectives  5.63 us (6%)
    all_gather x1, waiting for transfers between devices, gather_blocks(): parts = lax.all_gather(x, axis)  7.71 us
    all_to_all x1, starting transfers between devices, per_device(): lax.all_to_all(wanted.reshape(count_kv, 1), 'kv', split_axis=0, concat_ax...  7.31 us
    all_to_all x1, waiting for transfers between devices, per_device(): lax.all_to_all(outgoing, 'kv', split_axis=0, concat_axis=0, tiled=True)  6.5 us
    all_to_all x1, starting transfers between devices, per_device(): lax.all_to_all(outgoing, 'kv', split_axis=0, concat_axis=0, tiled=True)  6 us
    psum x1, blocking collectives, per_device(): squares = lax.psum(jnp.sum(attn_f32 * attn_f32, axis=1), 'tp')  5.63 us
    dot_general x4, matrix products, attend(): jnp.einsum('phqsk,pskd->pqhd', softmax_w, value_part, preferred_element_t...  4.94 us
    dynamic_slice x8, local copies, waits for them, and re-layouts, per_device(): lax.map(attend, (queries.reshape(pair_count, 2, BLK, head_count, HD), sel...  4.53 us
    dot_general x1, matrix products, per_device(): jnp.dot(gather_blocks(scaled, 'tp', 1), w_out, preferred_element_type=jnp...  2.75 us
  transfers between devices with their start and end apart: 3, of which 2 were waited for; matrix products, arithmetic and copies ran while one was open for 12% of the time, Pallas kernels for 0%

profile of v1, /device:TPU:0, one launch (start us, length us, event | category | flops | bytes accessed | tf_op | source)
XLA Modules:
  0.0 88.2 jit_solution(16616096739684033500)
XLA Ops:
  6.5 0.8 fusion.20
  8.9 7.3 %all-to-all-start = ((s32[8,1,1]{2,1,0:T(1,128)}), s32[8,1,1]{2,1,0:T(1,128)S(1)}, u32[]{:S(2)}, u32[]{:S(2)}) async-start(s32[8,1,1]{2,1,0:T(1,128)} %copy.39), calls=%async_computation | async-start | bytes 8192 | tf_op jit(solution)/shard_map/all_to_all | solution.py:68
  16.9 1.7 %convolution_bitcast_fusion.1 = f32[512,1,64]{0,2,1:T(8,128)S(1)} fusion(bf16[512,2048]{1,0:T(8,128)(2,1)S(1)} %copy-done, bf16[2048,64]{0,1:T(8,128)(2,1)} %param.11), kind=kOutput, calls=%fused_computation.26 | convolution fusion | flops 134217728 | bytes 2490368 | tf_op jit(solution)/shard_map/dot_general | solution.py:52
  20.4 2.0 %fusion.34 = f32[512,256]{0,1:T(8,128)S(1)} fusion(bf16[512,2048]{1,0:T(8,128)(2,1)S(1)} %copy-done, bf16[2048,256]{1,0:T(8,128)(2,1)} %param.10), kind=kOutput, calls=%fused_computation.93 | convolution fusion | flops 536870912 | bytes 3670016 | tf_op jit(solution)/shard_map/dot_general | solution.py:45
  22.9 1.6 %pad_maximum_fusion = bf16[4,2,64,4,64]{2,1,0,4,3:T(2,128)(2,1)} fusion(bf16[4,2,64,4,32]{2,1,0,4,3:T(2,128)(2,1)S(1)} %concatenate.35, bf16[4,2,64,4,32]{2,1,0,4,3:T(2,128)(2,1)S(1)} %concatenate.34), kind=kLoop, calls=%fused_computation.29 | loop fusion | flops 131072 | bytes 524288 | tf_op jit(solution)/shard_map/concatenate | solution.py:27
  26.6 6.0 %all-to-all-start.1 = ((bf16[8,64,128]{2,1,0:T(8,128)(2,1)}), bf16[8,64,128]{2,1,0:T(8,128)(2,1)S(1)}, u32[]{:S(2)}, u32[]{:S(2)}) async-start(bf16[8,64,128]{2,1,0:T(8,128)(2,1)} %broadcast_select_fusion), calls=%async_computation.1 | async-start | bytes 262144 | tf_op jit(solution)/shard_map/all_to_all | solution.py:76
  33.4 6.5 %all-to-all-done.1 = bf16[8,64,128]{2,1,0:T(8,128)(2,1)S(1)} async-done(((bf16[8,64,128]{2,1,0:T(8,128)(2,1)}), bf16[8,64,128]{2,1,0:T(8,128)(2,1)S(1)}, u32[]{:S(2)}, u32[]{:S(2)}) %all-to-all-start.1) | async-done | bytes 131104 | tf_op jit(solution)/shard_map/all_to_all | solution.py:76
  40.8 17.1 %while.11 = (s32[]{:T(128)}, bf16[4,2,64,4,64]{2,4,3,1,0:T(8,128)(2,1)}, bf16[4,2,8,64,128]{4,3,2,1,0:T(8,128)(2,1)S(1)}, pred[4,2,8]{2,1,0:T(4,128)(4,1)S(1)}, ...) while((s32[]{:T(128)}, ...), condition=%wide.region_4.5_spmd.clone, body=%wide.region_1.4_spmd.clone.sunk | while | flops 69369872 | bytes 13193617 | solution.py:105
  41.8 1.0 %constant_dynamic-slice_fusion.4 = bf16[1,2,64,4,64]{2,1,0,4,3:T(2,128)(2,1)S(1)} fusion(bf16[4,2,64,4,64]{2,1,0,4,3:T(2,128)(2,1)} %get-tuple-element.185, s32[]{:T(128)} %get-tuple-element.171), kind=kLoop, calls=%fused_computation.18.clone.1 | loop fusion | bytes 131076 | tf_op jit(solution)/shard_map/while/body/jit(dynamic_index_in_dim)/dynamic_slice | solution.py:105
  43.9 1.2 %fusion.52 = bf16[4,2,64,4,64]{2,4,3,1,0:T(8,128)(2,1)} fusion(bf16[4,2,64,4,64]{2,4,3,1,0:T(8,128)(2,1)} %get-tuple-element.172, s32[]{:T(128)} %get-tuple-element.171, f32[2,4,64,8,64]{2,4,1,3,0:T(8,128)S(1)} %get-tuple-element.161, f32[2,4,64]{2,1,0:T(4,128)S(1)} %fusion.51, f32[2,4,64]{2,1,0:T(4,128)S(1)} %get-tuple-element.162, ...), kind=kOutput, calls=%fused_computation.10.clone.1 | convolution fusion | flops 34373632 | bytes 1446400 | tf_op jit(solution)/shard_map/while/body/eval_jaxpr/phqsk,pskd->pqhd/dot_general | solution.py:100
  46.1 1.0 %constant_dynamic-slice_fusion.4 = bf16[1,2,64,4,64]{2,1,0,4,3:T(2,128)(2,1)S(1)} fusion(bf16[4,2,64,4,64]{2,1,0,4,3:T(2,128)(2,1)} %get-tuple-element.185, s32[]{:T(128)} %get-tuple-element.171), kind=kLoop, calls=%fused_computation.18.clone.1 | loop fusion | bytes 131076 | tf_op jit(solution)/shard_map/while/body/jit(dynamic_index_in_dim)/dynamic_slice | solution.py:105
  48.1 1.2 %fusion.52 = bf16[4,2,64,4,64]{2,4,3,1,0:T(8,128)(2,1)} fusion(bf16[4,2,64,4,64]{2,4,3,1,0:T(8,128)(2,1)} %get-tuple-element.172, s32[]{:T(128)} %get-tuple-element.171, f32[2,4,64,8,64]{2,4,1,3,0:T(8,128)S(1)} %get-tuple-element.161, f32[2,4,64]{2,1,0:T(4,128)S(1)} %fusion.51, f32[2,4,64]{2,1,0:T(4,128)S(1)} %get-tuple-element.162, ...), kind=kOutput, calls=%fused_computation.10.clone.1 | convolution fusion | flops 34373632 | bytes 1446400 | tf_op jit(solution)/shard_map/while/body/eval_jaxpr/phqsk,pskd->pqhd/dot_general | solution.py:100
  50.4 1.0 %constant_dynamic-slice_fusion.4 = bf16[1,2,64,4,64]{2,1,0,4,3:T(2,128)(2,1)S(1)} fusion(bf16[4,2,64,4,64]{2,1,0,4,3:T(2,128)(2,1)} %get-tuple-element.185, s32[]{:T(128)} %get-tuple-element.171), kind=kLoop, calls=%fused_computation.18.clone.1 | loop fusion | bytes 131076 | tf_op jit(solution)/shard_map/while/body/jit(dynamic_index_in_dim)/dynamic_slice | solution.py:105
  52.4 1.2 %fusion.52 = bf16[4,2,64,4,64]{2,4,3,1,0:T(8,128)(2,1)} fusion(bf16[4,2,64,4,64]{2,4,3,1,0:T(8,128)(2,1)} %get-tuple-element.172, s32[]{:T(128)} %get-tuple-element.171, f32[2,4,64,8,64]{2,4,1,3,0:T(8,128)S(1)} %get-tuple-element.161, f32[2,4,64]{2,1,0:T(4,128)S(1)} %fusion.51, f32[2,4,64]{2,1,0:T(4,128)S(1)} %get-tuple-element.162, ...), kind=kOutput, calls=%fused_computation.10.clone.1 | convolution fusion | flops 34373632 | bytes 1446400 | tf_op jit(solution)/shard_map/while/body/eval_jaxpr/phqsk,pskd->pqhd/dot_general | solution.py:100
  54.7 1.0 %constant_dynamic-slice_fusion.4 = bf16[1,2,64,4,64]{2,1,0,4,3:T(2,128)(2,1)S(1)} fusion(bf16[4,2,64,4,64]{2,1,0,4,3:T(2,128)(2,1)} %get-tuple-element.185, s32[]{:T(128)} %get-tuple-element.171), kind=kLoop, calls=%fused_computation.18.clone.1 | loop fusion | bytes 131076 | tf_op jit(solution)/shard_map/while/body/jit(dynamic_index_in_dim)/dynamic_slice | solution.py:105
  56.7 1.2 %fusion.52 = bf16[4,2,64,4,64]{2,4,3,1,0:T(8,128)(2,1)} fusion(bf16[4,2,64,4,64]{2,4,3,1,0:T(8,128)(2,1)} %get-tuple-element.172, s32[]{:T(128)} %get-tuple-element.171, f32[2,4,64,8,64]{2,4,1,3,0:T(8,128)S(1)} %get-tuple-element.161, f32[2,4,64]{2,1,0:T(4,128)S(1)} %fusion.51, f32[2,4,64]{2,1,0:T(4,128)S(1)} %get-tuple-element.162, ...), kind=kOutput, calls=%fused_computation.10.clone.1 | convolution fusion | flops 34373632 | bytes 1446400 | tf_op jit(solution)/shard_map/while/body/eval_jaxpr/phqsk,pskd->pqhd/dot_general | solution.py:100
  57.9 1.3 %copy.44 = f32[4,2,64,4,64]{4,3,2,1,0:T(4,128)S(1)} copy(bf16[4,2,64,4,64]{2,4,3,1,0:T(8,128)(2,1)} %get-tuple-element.47) | data formatting | bytes 786432 | tf_op jit(solution)/shard_map/convert_element_type | solution.py:115
  59.3 1.4 %reshape.395 = f32[1,512,256]{2,1,0:T(8,128)} reshape(f32[4,2,64,4,64]{4,3,2,1,0:T(4,128)S(1)} %copy.44) | data formatting | bytes 1048576 | tf_op jit(solution)/shard_map/convert_element_type | solution.py:115
  60.7 1.8 %multiply_convert_fusion = bf16[1,512,256]{2,1,0:T(8,128)(2,1)} fusion(f32[1,512,256]{2,1,0:T(8,128)} %reshape.395, f32[256]{0:T(256)S(1)} %dynamic_slice.23), kind=kLoop, calls=%fused_computation.30 | loop fusion | flops 262144 | bytes 787456 | tf_op jit(solution)/shard_map/convert_element_type | solution.py:118
  62.5 1.2 %multiply_reduce_fusion = f32[4,2,64]{2,1,0:T(2,128)S(1)} fusion(bf16[4,2,64,4,64]{2,4,3,1,0:T(8,128)(2,1)} %get-tuple-element.47), kind=kLoop, calls=%fused_computation.28 | loop fusion | flops 392704 | bytes 264192 | tf_op jit(solution)/shard_map/reduce_sum | solution.py:116
  63.8 5.6 %psum.7 = f32[512]{0:T(512)S(1)} all-reduce(f32[512]{0:T(512)S(1)} %reduce_sum.21), channel_id=1, replica_groups=mesh['kv'=8,'tp'=4] {'tp'}, use_global_device_ids=true, to_apply=%region_6.7 | all-reduce | flops 512 | bytes 4096 | tf_op jit(solution)/shard_map/psum | solution.py:116
  69.4 7.7 %all-gather.2.cloned.1.call-done = bf16[4,512,256]{2,1,0:T(8,128)(2,1)} async-done(((bf16[1,512,256]{2,1,0:T(8,128)(2,1)}), bf16[4,512,256]{2,1,0:T(8,128)(2,1)}) %all-gather.2.cloned.1.call-update) | async-done | bytes 1048592 | tf_op jit(solution)/shard_map/all_gather | solution.py:15
  77.1 1.5 %copy.45 = bf16[4,512,256]{1,2,0:T(8,128)(2,1)S(1)} copy(bf16[4,512,256]{2,1,0:T(8,128)(2,1)} %all-gather.2.cloned.1.call-done) | data formatting | bytes 2097152 | tf_op jit(solution)/shard_map/all_gather | solution.py:15
  78.6 2.8 %fusion.10 = bf16[512,512]{1,0:T(8,128)(2,1)} fusion(bf16[512,1024]{0,1:T(8,128)(2,1)S(1)} %bitcast.158, bf16[1024,512]{1,0:T(8,128)(2,1)} %param.13, f32[512]{0:T(512)S(1)} %add_rsqrt_fusion), kind=kOutput, calls=%fused_computation.25 | convolution fusion | flops 537395200 | bytes 2623488 | tf_op jit(solution)/shard_map/dot_general | solution.py:119
  (92 shorter events, 16.2 us)
Async XLA Ops:
  6.5 10.4 %copy-start = (bf16[512,2048]{1,0:T(8,128)(2,1)S(1)}, bf16[512,2048]{1,0:T(8,128)(2,1)}, u32[]{:S(2)}) copy-start(bf16[512,2048]{1,0:T(8,128)(2,1)} %param.9) | copy-start | bytes 6291460
  6.5 13.0 %copy-start.3 = (bf16[2048,64]{0,1:T(8,128)(2,1)S(1)}, bf16[2048,64]{0,1:T(8,128)(2,1)}, u32[]{:S(2)}) copy-start(bf16[2048,64]{0,1:T(8,128)(2,1)} %param.12) | copy-start | bytes 786436
  8.9 15.9 %all-to-all-start = ((s32[8,1,1]{2,1,0:T(1,128)}), s32[8,1,1]{2,1,0:T(1,128)S(1)}, u32[]{:S(2)}, u32[]{:S(2)}) async-start(s32[8,1,1]{2,1,0:T(1,128)} %copy.39), calls=%async_computation | async-start | bytes 8192 | tf_op jit(solution)/shard_map/all_to_all | solution.py:68
  22.4 11.0 %copy-start.4 = (s32[1,8,8]{2,1,0:T(8,128)S(1)}, s32[1,8,8]{2,1,0:T(8,128)}, u32[]{:S(2)}) copy-start(s32[1,8,8]{2,1,0:T(8,128)} %param.15) | copy-start | bytes 772
  26.6 13.3 %all-to-all-start.1 = ((bf16[8,64,128]{2,1,0:T(8,128)(2,1)}), bf16[8,64,128]{2,1,0:T(8,128)(2,1)S(1)}, u32[]{:S(2)}, u32[]{:S(2)}) async-start(bf16[8,64,128]{2,1,0:T(8,128)(2,1)} %broadcast_select_fusion), calls=%async_computation.1 | async-start | bytes 262144 | tf_op jit(solution)/shard_map/all_to_all | solution.py:76
  32.6 44.6 %all-gather.2.cloned.1.call-start = ((), (), s32[]{:S(2)}) async-start(), calls=%async_computation.2 | async-start | bytes 1310720 | tf_op jit(solution)/shard_map/all_gather | solution.py:15
  40.8 1.0 %copy-start.1 = (bf16[4,2,8,64,128]{4,3,2,1,0:T(8,128)(2,1)}, bf16[4,2,8,64,128]{4,3,2,1,0:T(8,128)(2,1)S(1)}, u32[]{:S(2)}) copy-start(bf16[4,2,8,64,128]{4,3,2,1,0:T(8,128)(2,1)S(1)} %get-tuple-element.181) | copy-start | bytes 3145732 | tf_op jit(solution)/shard_map/while
  43.9 1.2 %copy-start.2 = (bf16[4,2,8,64,128]{4,3,2,1,0:T(8,128)(2,1)S(1)}, bf16[4,2,8,64,128]{4,3,2,1,0:T(8,128)(2,1)}, u32[]{:S(2)}) copy-start(bf16[4,2,8,64,128]{4,3,2,1,0:T(8,128)(2,1)} %copy-done.1) | copy-start | bytes 3145732 | tf_op jit(solution)/shard_map/while
  45.1 1.0 %copy-start.1 = (bf16[4,2,8,64,128]{4,3,2,1,0:T(8,128)(2,1)}, bf16[4,2,8,64,128]{4,3,2,1,0:T(8,128)(2,1)S(1)}, u32[]{:S(2)}) copy-start(bf16[4,2,8,64,128]{4,3,2,1,0:T(8,128)(2,1)S(1)} %get-tuple-element.181) | copy-start | bytes 3145732 | tf_op jit(solution)/shard_map/while
  48.1 1.2 %copy-start.2 = (bf16[4,2,8,64,128]{4,3,2,1,0:T(8,128)(2,1)S(1)}, bf16[4,2,8,64,128]{4,3,2,1,0:T(8,128)(2,1)}, u32[]{:S(2)}) copy-start(bf16[4,2,8,64,128]{4,3,2,1,0:T(8,128)(2,1)} %copy-done.1) | copy-start | bytes 3145732 | tf_op jit(solution)/shard_map/while
  49.4 1.0 %copy-start.1 = (bf16[4,2,8,64,128]{4,3,2,1,0:T(8,128)(2,1)}, bf16[4,2,8,64,128]{4,3,2,1,0:T(8,128)(2,1)S(1)}, u32[]{:S(2)}) copy-start(bf16[4,2,8,64,128]{4,3,2,1,0:T(8,128)(2,1)S(1)} %get-tuple-element.181) | copy-start | bytes 3145732 | tf_op jit(solution)/shard_map/while
  52.4 1.2 %copy-start.2 = (bf16[4,2,8,64,128]{4,3,2,1,0:T(8,128)(2,1)S(1)}, bf16[4,2,8,64,128]{4,3,2,1,0:T(8,128)(2,1)}, u32[]{:S(2)}) copy-start(bf16[4,2,8,64,128]{4,3,2,1,0:T(8,128)(2,1)} %copy-done.1) | copy-start | bytes 3145732 | tf_op jit(solution)/shard_map/while
  53.7 1.0 %copy-start.1 = (bf16[4,2,8,64,128]{4,3,2,1,0:T(8,128)(2,1)}, bf16[4,2,8,64,128]{4,3,2,1,0:T(8,128)(2,1)S(1)}, u32[]{:S(2)}) copy-start(bf16[4,2,8,64,128]{4,3,2,1,0:T(8,128)(2,1)S(1)} %get-tuple-element.181) | copy-start | bytes 3145732 | tf_op jit(solution)/shard_map/while
  56.7 1.2 %copy-start.2 = (bf16[4,2,8,64,128]{4,3,2,1,0:T(8,128)(2,1)S(1)}, bf16[4,2,8,64,128]{4,3,2,1,0:T(8,128)(2,1)}, u32[]{:S(2)}) copy-start(bf16[4,2,8,64,128]{4,3,2,1,0:T(8,128)(2,1)} %copy-done.1) | copy-start | bytes 3145732 | tf_op jit(solution)/shard_map/while
Sparse Core Ops, SparseCore 0:
  62.6 14.4 all-gather.1
